TPU v7x, 32 devices: a whole 2x2x4 slice. The times are simulated.
32 devices in a mesh: sp: 16 (over z, y, x), tp: 2 (over core).
Axes of the slice: x: 2, y: 2, z: 4, core: 2. Of those that a mesh axis runs over, the one named last changes fastest.
Arguments:
- queries: bfloat16 [3072, 1024], P('sp', 'tp'), may hold values from -6 to 6
- keys: bfloat16 [3072, 512], P('sp', 'tp'), may hold values from -6 to 6
- values: bfloat16 [3072, 512], P('sp', 'tp'), may hold values from -6 to 6
- query_gain: float32 [16, 64], P('tp'), may hold values from 1.4 to 7.5
- key_gain: float32 [8, 64], P('tp'), may hold values from 1.4 to 7.5
- out_weight: bfloat16 [1024, 2048], P('tp'), may hold values from -0.375 to 0.375
- residual: bfloat16 [3072, 2048], P('sp'), may hold values from -170 to 170
- norm_gain: float32 [2048], replicated, may hold values from 0.1 to 1.9
- gate_weight: bfloat16 [2048, 5632], P('sp', 'tp'), may hold values from -0.125 to 0.125
- up_weight: bfloat16 [2048, 5632], P('sp', 'tp'), may hold values from -0.125 to 0.125
- down_weight: bfloat16 [5632, 2048], P('tp', 'sp'), may hold values from -0.15625 to 0.15625
Outputs:
- mixed: bfloat16 [3072, 2048], P('sp')
All inputs are finite; a program needn't handle non-finite values.
Results may differ from a plain program's by a relative error of at most 0.017.
Values may be sent and summed in bfloat16 or wider, within the bound.
A program may use at most 128 MiB of HBM per device.

v0:
```python
import jax
import jax.numpy as jnp
from jax import lax
from jax.sharding import PartitionSpec as P

GRID_W = 64
epsilon = 1e-06
rope_base = 10000.0
block_keys = 2048


def rotate_pairs(entries, places):
    half = entries.shape[-1] // 2
    frequency = rope_base ** (-jnp.arange(half, dtype=jnp.float32) / half)
    angle = places.astype(jnp.float32)[:, None, None] * frequency[None, None, :]
    cosine = jnp.cos(angle)
    sine = jnp.sin(angle)
    first = entries[..., :half]
    second = entries[..., half:]
    return jnp.concatenate(
        [first * cosine - second * sine, first * sine + second * cosine], axis=-1
    )


def grid_rotate(entries, grid_rows, grid_cols):
    half = entries.shape[-1] // 2
    return jnp.concatenate(
        [
            rotate_pairs(entries[..., :half], grid_rows),
            rotate_pairs(entries[..., half:], grid_cols),
        ],
        axis=-1,
    )


def head_norm(entries, gains):
    factor = lax.rsqrt(jnp.mean(entries * entries, axis=-1, keepdims=True) + epsilon)
    return entries * factor * gains[None]


def row_norm(mid, norm_gain):
    wide = mid.astype(jnp.float32)
    return (
        wide * lax.rsqrt(jnp.mean(wide * wide, axis=-1, keepdims=True) + epsilon) * norm_gain
    ).astype(jnp.bfloat16)


def block_span(length):
    if length <= block_keys:
        return length
    span = block_keys
    while length % span != 0:
        span = span - 1
    return span


def body(
    queries,
    keys,
    values,
    query_gain,
    key_gain,
    out_weight,
    residual,
    norm_gain,
    gate_weight,
    up_weight,
    down_weight,
):
    own = queries.shape[0]
    heads = query_gain.shape[0]
    key_heads = key_gain.shape[0]
    head_size = query_gain.shape[1]
    group = heads // key_heads
    gate_full, up_full, down_full = (
        lax.all_gather(gate_weight, "sp", axis=0, tiled=True),
        lax.all_gather(up_weight, "sp", axis=0, tiled=True),
        lax.all_gather(down_weight, "sp", axis=1, tiled=True),
    )
    places = lax.axis_index("sp") * own + jnp.arange(own, dtype=jnp.int32)
    grid_rows = places // GRID_W
    grid_cols = places % GRID_W
    query_turned = grid_rotate(
        head_norm(queries.astype(jnp.float32).reshape(own, heads, head_size), query_gain),
        grid_rows,
        grid_cols,
    ).astype(jnp.bfloat16)
    query_groups = query_turned.reshape(own, key_heads, group, head_size)
    key_turned = (
        grid_rotate(
            head_norm(keys.astype(jnp.float32).reshape(own, key_heads, head_size), key_gain),
            grid_rows,
            grid_cols,
        )
        .astype(jnp.bfloat16)
        .reshape(own, key_heads * head_size)
    )
    scale = head_size ** (-0.5)

    def absorb(carry, key_block, value_block):
        top, total, summed = carry
        key_block = key_block.reshape(-1, key_heads, head_size)
        value_block = value_block.reshape(-1, key_heads, head_size)
        score = (
            jnp.einsum(
                "qgrd,kgd->qgrk", query_groups, key_block, preferred_element_type=jnp.float32
            )
            * scale
        )
        new_top = jnp.maximum(top, jnp.max(score, axis=-1))
        weight = jnp.exp(score - new_top[..., None])
        shrink = jnp.exp(top - new_top)
        total = total * shrink + jnp.sum(weight, axis=-1)
        summed = summed * shrink[..., None] + jnp.einsum(
            "qgrk,kgd->qgrd",
            weight.astype(jnp.bfloat16),
            value_block,
            preferred_element_type=jnp.float32,
        )
        return (new_top, total, summed)

    def fold_keys(carry, pieces):
        length = pieces[0].shape[0]
        span = block_span(length)
        if span == length:
            return absorb(carry, pieces[0], pieces[1])
        width = pieces[0].shape[1]
        key_blocks = pieces[0].reshape(length // span, span, width)
        value_blocks = pieces[1].reshape(length // span, span, width)

        def scan_step(inner, blocks):
            return (absorb(inner, blocks[0], blocks[1]), None)

        result, unused = lax.scan(scan_step, carry, (key_blocks, value_blocks))
        return result

    start_state = (
        jnp.full((own, key_heads, group), -jnp.inf, jnp.float32),
        jnp.zeros((own, key_heads, group), jnp.float32),
        jnp.zeros((own, key_heads, group, head_size), jnp.float32),
    )
    top, total, summed = fold_keys(
        start_state,
        (
            lax.all_gather(key_turned, "sp", axis=0, tiled=True),
            lax.all_gather(values, "sp", axis=0, tiled=True),
        ),
    )
    attended = (summed / total[..., None]).reshape(own, heads * head_size).astype(jnp.bfloat16)
    part_rows = own // lax.axis_size("tp")
    branch = lax.psum_scatter(
        jnp.dot(
            lax.slice_in_dim(attended, 0, lax.axis_size("tp") * part_rows, axis=0),
            out_weight,
            preferred_element_type=jnp.float32,
        ).astype(jnp.bfloat16),
        "tp",
        scatter_dimension=0,
        tiled=True,
    ).astype(jnp.float32)
    own_rows = lax.dynamic_slice_in_dim(residual, lax.axis_index("tp") * part_rows, part_rows, 0)
    mid = (own_rows.astype(jnp.float32) + branch).astype(jnp.bfloat16)
    normed_all = lax.all_gather(row_norm(mid, norm_gain), "tp", axis=0, tiled=True)
    gate = jnp.dot(normed_all, gate_full, preferred_element_type=jnp.float32)
    up_value = jnp.dot(normed_all, up_full, preferred_element_type=jnp.float32)
    hidden = (jax.nn.silu(gate) * up_value).astype(jnp.bfloat16)
    terms = jnp.dot(hidden, down_full, preferred_element_type=jnp.float32)
    ffn = lax.psum_scatter(
        terms.astype(jnp.bfloat16), "tp", scatter_dimension=0, tiled=True
    ).astype(jnp.float32)
    finished = (mid.astype(jnp.float32) + ffn).astype(jnp.bfloat16)
    return lax.all_gather(finished, "tp", axis=0, tiled=True)


def solution(mesh):
    in_specs = (
        P("sp", "tp"),
        P("sp", "tp"),
        P("sp", "tp"),
        P("tp", None),
        P("tp", None),
        P("tp", None),
        P("sp", None),
        P(),
        P("sp", "tp"),
        P("sp", "tp"),
        P("tp", "sp"),
    )
    out_specs = P("sp", None)
    return jax.shard_map(body, mesh=mesh, in_specs=in_specs, out_specs=out_specs, check_vma=False)
```

profile of v0, /device:TPU:0, one launch (start us, length us, event | category | flops | bytes accessed | tf_op | source)
XLA Modules:
  0.0 684.2 jit_solution(15495165526293549305)
XLA Ops:
  6.6 1.1 copy.22
  7.8 0.8 fusion.22
  8.6 0.2 multiply_cosine_fusion.1
  8.8 0.7 copy.23
  9.6 0.0 all-gather.8.cloned.1.call-start
  9.7 0.7 all-gather.8.cloned.1.call-update
  10.4 0.0 reduce-scatter.3.cloned.1.call-start
  10.4 1.1 copy.24
  11.5 0.1 fusion.19
  11.6 0.8 fusion.20
  12.4 0.1 subtract_convert_fusion.1
  12.5 0.7 pad_maximum_fusion
  13.3 57.5 %all-gather.6.cloned.1.call-done = bf16[3072,256]{1,0:T(8,128)(2,1)} async-done(((bf16[192,256]{1,0:T(8,128)(2,1)}), bf16[3072,256]{1,0:T(8,128)(2,1)}) %all-gather.6.cloned.1.call-update) | async-done | bytes 1572880 | tf_op jit(solution)/shard_map/all_gather | solution.py:145
  70.8 59.5 %all-gather.8.cloned.1.call-done = bf16[3072,256]{1,0:T(8,128)(2,1)} async-done(((bf16[192,256]{1,0:T(8,128)(2,1)}), bf16[3072,256]{1,0:T(8,128)(2,1)}) %all-gather.8.cloned.1.call-update) | async-done | bytes 1572880 | tf_op jit(solution)/shard_map/all_gather | solution.py:146
  130.3 43.6 %while.15 = (s32[]{:T(128)}, f32[192,4,2]{0,2,1:T(2,128)S(1)}, f32[192,4,2]{0,2,1:T(2,128)S(1)}, f32[192,4,2,64]{0,3,2,1:T(8,128)S(1)}, bf16[2,1536,256]{2,1,0:T...) while((s32[]{:T(128)}, f32[192,4,2]{0,2,1:T(2,128)S(1)}, ...), condition=%wide.region_5.6_spmd.clone, body=%wide.region_2.5_spmd.clone.sunk | while | flops 623156736 | bytes 37257324 | solution.py:134
  130.3 2.6 constant_dynamic-slice_fusion.3
  132.9 1.4 copy.33
  134.3 6.0 bitcast_reduce_fusion.2
  140.4 5.4 fusion.51
  145.8 1.4 copy.34
  147.2 4.8 fusion.53
  152.1 2.6 constant_dynamic-slice_fusion.3
  154.7 1.4 copy.33
  156.1 6.0 bitcast_reduce_fusion.2
  162.1 5.4 fusion.51
  167.6 1.4 copy.34
  169.0 4.8 fusion.53
  173.9 0.1 divide_convert_fusion
  173.9 1.5 convolution_convert_fusion.1
  175.4 0.0 all-gather.10.cloned.1.call-start
  175.5 0.5 all-gather.10.cloned.1.call-update
  176.0 0.0 all-gather.12.cloned.1.call-start
  176.1 0.5 all-gather.12.cloned.1.call-update
  176.7 0.5 all-gather.14.cloned.1.call-update
  177.2 0.0 reduce-scatter.5.cloned.1.call-start
  177.2 5.2 reduce-scatter.3.cloned.1.call-done
  182.5 1.4 fusion.15
  183.9 0.2 fusion.17
  184.0 2.5 all_gather.23
  186.6 141.1 %all-gather.10.cloned.1.call-done = bf16[2048,2816]{1,0:T(8,128)(2,1)} async-done(((bf16[128,2816]{1,0:T(8,128)(2,1)}), bf16[2048,2816]{1,0:T(8,128)(2,1)}) %all-gather.10.cloned.1.call-update) | async-done | bytes 11534352 | tf_op jit(solution)/shard_map/all_gather | solution.py:76
  327.6 8.0 %fusion.27 = f32[192,2816]{1,0:T(8,128)} fusion(bf16[192,2048]{1,0:T(8,128)(2,1)S(1)} %all_gather.23, bf16[2048,2816]{1,0:T(8,128)(2,1)} %all-gather.10.cloned.1.call-done), kind=kOutput, calls=%fused_computation.67 | convolution fusion | flops 2214592512 | bytes 14483456 | tf_op jit(solution)/shard_map/dot_general | solution.py:164
  335.7 134.2 %all-gather.12.cloned.1.call-done = bf16[2048,2816]{1,0:T(8,128)(2,1)} async-done(((bf16[128,2816]{1,0:T(8,128)(2,1)}), bf16[2048,2816]{1,0:T(8,128)(2,1)}) %all-gather.12.cloned.1.call-update) | async-done | bytes 11534352 | tf_op jit(solution)/shard_map/all_gather | solution.py:77
  469.9 182.8 %all-gather.14.cloned.1.call-done = bf16[2816,2048]{1,0:T(8,128)(2,1)} async-done(((bf16[2816,128]{1,0:T(8,128)(2,1)}), bf16[2816,2048]{1,0:T(8,128)(2,1)}) %all-gather.14.cloned.1.call-update) | async-done | bytes 11534352 | tf_op jit(solution)/shard_map/all_gather | solution.py:78
  652.7 13.8 %convolution_convert_fusion = bf16[192,2048]{1,0:T(8,128)(2,1)} fusion(bf16[2816,2048]{1,0:T(8,128)(2,1)} %all-gather.14.cloned.1.call-done, bf16[192,2048]{1,0:T(8,128)(2,1)S(1)} %all_gather.23, bf16[2048,2816]{1,0:T(8,128)(2,1)} %all-gather.12.cloned.1.call-done, f32[192,2816]{1,0:T(8,128)} %fusion.27), kind=kOutput, calls=%fused_computation.19 | convolution fusion | flops 4432822272 | bytes 26804224 | tf_op jit(solution)/shard_map/dot_general | solution.py:167
  666.5 6.5 reduce-scatter.5.cloned.1.call-done
  673.0 1.1 fusion.18
  674.1 2.4 all_gather.27
  676.5 0.9 copy.48
  (26 shorter events, 0.3 us)
Async XLA Ops:
  6.5 167.4 %copy-start = (bf16[512,2048]{1,0:T(8,128)(2,1)S(1)}, bf16[512,2048]{1,0:T(8,128)(2,1)}, u32[]{:S(2)}) copy-start(bf16[512,2048]{1,0:T(8,128)(2,1)} %param.18) | copy-start | bytes 6291460
  6.5 64.3 %all-gather.6.cloned.1.call-start = ((), (), s32[]{:S(2)}) async-start(), calls=%async_computation.2 | async-start | bytes 1671168 | tf_op jit(solution)/shard_map/all_gather | solution.py:145
  9.6 120.7 %all-gather.8.cloned.1.call-start = ((), (), s32[]{:S(2)}) async-start(), calls=%async_computation.3 | async-start | bytes 1671168 | tf_op jit(solution)/shard_map/all_gather | solution.py:146
  10.4 172.1 %reduce-scatter.3.cloned.1.call-start = ((), (), s32[]{:S(2)}) async-start(), calls=%async_computation.4 | async-start | bytes 1179648 | tf_op jit(solution)/shard_map/reduce_scatter | solution.py:151
  130.3 53.6 %copy-start.1 = (f32[2048]{0:T(1024)S(1)}, f32[2048]{0:T(1024)}, u32[]{:S(2)}) copy-start(f32[2048]{0:T(1024)} %param.20) | copy-start | bytes 24580
  175.4 152.2 %all-gather.10.cloned.1.call-start = ((), (), s32[]{:S(2)}) async-start(), calls=%async_computation.5 | async-start | bytes 12255232 | tf_op jit(solution)/shard_map/all_gather | solution.py:76
  176.0 293.9 %all-gather.12.cloned.1.call-start = ((), (), s32[]{:S(2)}) async-start(), calls=%async_computation.6 | async-start | bytes 12255232 | tf_op jit(solution)/shard_map/all_gather | solution.py:77
  176.6 476.1 %all-gather.14.cloned.1.call-start = ((), (), s32[]{:S(2)}) async-start(), calls=%async_computation.7 | async-start | bytes 12255232 | tf_op jit(solution)/shard_map/all_gather | solution.py:78
  177.2 495.9 %reduce-scatter.5.cloned.1.call-start = ((), (), s32[]{:S(2)}) async-start(), calls=%async_computation.8 | async-start | bytes 1179648 | tf_op jit(solution)/shard_map/reduce_scatter | solution.py:168
Sparse Core Ops, SparseCore 0:
  10.1 60.6 all-gather.5
  73.6 56.6 all-gather.7
  175.6 6.8 reduce-scatter.2
  185.1 142.5 all-gather.9
  330.2 139.5 all-gather.11
  472.4 180.2 all-gather.13
  666.7 6.3 reduce-scatter.4
where the time goes:
time: 685 us; the launch traced here: 684 us
  waiting for transfers between devices  589 us (86%)
  matrix products  45.1 us (7%)
  other arithmetic  16.4 us (2%)
  local copies, waits for them, and re-layouts  14.7 us (2%)
  between operations  13.7 us (2%)
    all_gather x1, waiting for transfers between devices, body(): lax.all_gather(down_weight, 'sp', axis=1, tiled=True)  183 us
    all_gather x1, waiting for transfers between devices, body(): lax.all_gather(gate_weight, 'sp', axis=0, tiled=True)  141 us
    all_gather x1, waiting for transfers between devices, body(): lax.all_gather(up_weight, 'sp', axis=0, tiled=True)  134 us
    all_gather x1, waiting for transfers between devices, body(): lax.all_gather(values, 'sp', axis=0, tiled=True)  59.5 us
    all_gather x1, waiting for transfers between devices, body(): lax.all_gather(key_turned, 'sp', axis=0, tiled=True)  57.5 us
    dot_general x1, matrix products, body(): terms = jnp.dot(hidden, down_full, preferred_element_type=jnp.float32)  13.8 us
  transfers between devices with their start and end apart: 7, of which 7 were waited for; matrix products, arithmetic and copies ran while one was open for 2% of the time, Pallas kernels for 0%

commit v1 on v0

--- a/solution.py
+++ b/solution.py
@@ -7,6 +7,11 @@
 epsilon = 1e-06
 rope_base = 10000.0
 block_keys = 2048
+
+
+def stack_and_merge(shard, name, dim):
+    shards = lax.all_gather(shard, name)
+    return jnp.concatenate(shards, axis=dim)
 
 
 def rotate_pairs(entries, places):
@@ -75,7 +80,7 @@
     gate_full, up_full, down_full = (
         lax.all_gather(gate_weight, "sp", axis=0, tiled=True),
         lax.all_gather(up_weight, "sp", axis=0, tiled=True),
-        lax.all_gather(down_weight, "sp", axis=1, tiled=True),
+        stack_and_merge(down_weight, "sp", 1),
     )
     places = lax.axis_index("sp") * own + jnp.arange(own, dtype=jnp.int32)
     grid_rows = places // GRID_W

time: 685 us -> 646 us (0.943)
  waiting for transfers between devices: 589 us -> 533 us
  local copies, waits for them, and re-layouts: 14.7 us -> 29.9 us
    all_gather x1, waiting for transfers between devices: 183 us -> 141 us  [stack_and_merge(): shards = lax.all_gather(shard, name)]
    reshape x0 -> x1, local copies, waits for them, and re-layouts: none -> 15.2 us  [stack_and_merge(): return jnp.concatenate(shards, axis=dim)]
    all_gather x1, waiting for transfers between devices: 141 us -> 127 us  [body(): lax.all_gather(gate_weight, 'sp', axis=0, tiled=True)]
  transfers between devices with their start and end apart: 7 -> 7, of which waited for: 7 -> 7; matrix products, arithmetic and copies ran while one was open for 2% -> 4% of each run, Pallas kernels for 0% -> 0%
where the time goes in v1:
time: 646 us; the launch traced here: 645 us
  waiting for transfers between devices  533 us (83%)
  matrix products  46.5 us (7%)
  local copies, waits for them, and re-layouts  29.9 us (5%)
  other arithmetic  16.4 us (3%)
  between operations  13.7 us (2%)
    all_gather x1, waiting for transfers between devices, stack_and_merge(): shards = lax.all_gather(shard, name)  141 us
    all_gather x1, waiting for transfers between devices, body(): lax.all_gather(up_weight, 'sp', axis=0, tiled=True)  134 us
    all_gather x1, waiting for transfers between devices, body(): lax.all_gather(gate_weight, 'sp', axis=0, tiled=True)  127 us
    all_gather x1, waiting for transfers between devices, body(): lax.all_gather(values, 'sp', axis=0, tiled=True)  59.5 us
    all_gather x1, waiting for transfers between devices, body(): lax.all_gather(key_turned, 'sp', axis=0, tiled=True)  57.5 us
    dot_general x1, matrix products, body(): terms = jnp.dot(hidden, down_full, preferred_element_type=jnp.float32)  15.2 us
    reshape x1, local copies, waits for them, and re-layouts, stack_and_merge(): return jnp.concatenate(shards, axis=dim)  15.2 us
  transfers between devices with their start and end apart: 7, of which 7 were waited for; matrix products, arithmetic and copies ran while one was open for 4% of the time, Pallas kernels for 0%

profile of v1, /device:TPU:0, one launch (start us, length us, event | category | flops | bytes accessed | tf_op | source)
XLA Modules:
  0.0 645.1 jit_solution(5440576227658186768)
XLA Ops:
  6.6 1.1 copy.28
  7.8 0.8 fusion.22
  8.6 0.2 multiply_cosine_fusion.1
  8.8 0.7 copy.29
  9.6 0.0 all-gather.9.cloned.1.call-start
  9.7 0.7 all-gather.9.cloned.1.call-update
  10.4 0.0 reduce-scatter.3.cloned.1.call-start
  10.4 1.1 copy.30
  11.5 0.1 fusion.19
  11.6 0.8 fusion.20
  12.4 0.1 subtract_convert_fusion.1
  12.5 0.7 pad_maximum_fusion
  13.3 57.5 %all-gather.7.cloned.1.call-done = bf16[3072,256]{1,0:T(8,128)(2,1)} async-done(((bf16[192,256]{1,0:T(8,128)(2,1)}), bf16[3072,256]{1,0:T(8,128)(2,1)}) %all-gather.7.cloned.1.call-update) | async-done | bytes 1572880 | tf_op jit(solution)/shard_map/all_gather | solution.py:150
  70.8 59.5 %all-gather.9.cloned.1.call-done = bf16[3072,256]{1,0:T(8,128)(2,1)} async-done(((bf16[192,256]{1,0:T(8,128)(2,1)}), bf16[3072,256]{1,0:T(8,128)(2,1)}) %all-gather.9.cloned.1.call-update) | async-done | bytes 1572880 | tf_op jit(solution)/shard_map/all_gather | solution.py:151
  130.3 43.6 %while.15 = (s32[]{:T(128)}, f32[192,4,2]{0,2,1:T(2,128)S(1)}, f32[192,4,2]{0,2,1:T(2,128)S(1)}, f32[192,4,2,64]{0,3,2,1:T(8,128)S(1)}, bf16[2,1536,256]{2,1,0:T...) while((s32[]{:T(128)}, f32[192,4,2]{0,2,1:T(2,128)S(1)}, ...), condition=%wide.region_5.6_spmd.clone, body=%wide.region_2.5_spmd.clone.sunk | while | flops 623156736 | bytes 37257324 | solution.py:139
  130.3 2.6 constant_dynamic-slice_fusion.3
  132.9 1.4 copy.40
  134.3 6.0 bitcast_reduce_fusion.2
  140.4 5.4 fusion.51
  145.8 1.4 copy.41
  147.2 4.8 fusion.53
  152.1 2.6 constant_dynamic-slice_fusion.3
  154.7 1.4 copy.40
  156.1 6.0 bitcast_reduce_fusion.2
  162.1 5.4 fusion.51
  167.6 1.4 copy.41
  169.0 4.8 fusion.53
  173.9 0.1 divide_convert_fusion
  173.9 1.5 convolution_convert_fusion.1
  175.4 0.0 all-gather.15.cloned.1.call-start
  175.5 0.5 all-gather.15.cloned.1.call-update
  176.1 0.5 all-gather.11.cloned.1.call-update
  176.7 0.5 all-gather.13.cloned.1.call-update
  177.2 0.0 reduce-scatter.5.cloned.1.call-start
  177.2 5.2 reduce-scatter.3.cloned.1.call-done
  182.5 1.4 fusion.15
  183.9 0.2 fusion.17
  184.0 2.5 all_gather.26
  186.6 141.1 %all-gather.15.cloned.1.call-done = bf16[45056,128]{1,0:T(8,128)(2,1)} async-done(((bf16[2816,128]{1,0:T(8,128)(2,1)}), bf16[45056,128]{1,0:T(8,128)(2,1)}) %all-gather.15.cloned.1.call-update) | async-done | bytes 11534352 | tf_op jit(solution)/shard_map/all_gather | solution.py:13
  327.6 15.2 %copy.33 = bf16[2816,16,128]{0,2,1:T(8,128)(2,1)} copy(bf16[2816,16,128]{2,0,1:T(8,128)(2,1)} %bitcast.78) | data formatting | bytes 23068672 | tf_op jit(solution)/shard_map/reshape | solution.py:14
  342.8 127.1 %all-gather.11.cloned.1.call-done = bf16[2048,2816]{1,0:T(8,128)(2,1)} async-done(((bf16[128,2816]{1,0:T(8,128)(2,1)}), bf16[2048,2816]{1,0:T(8,128)(2,1)}) %all-gather.11.cloned.1.call-update) | async-done | bytes 11534352 | tf_op jit(solution)/shard_map/all_gather | solution.py:81
  469.9 8.0 %fusion.27 = f32[192,2816]{1,0:T(8,128)} fusion(bf16[192,2048]{1,0:T(8,128)(2,1)S(1)} %all_gather.26, bf16[2048,2816]{1,0:T(8,128)(2,1)} %all-gather.11.cloned.1.call-done), kind=kOutput, calls=%fused_computation.67 | convolution fusion | flops 2214592512 | bytes 14483456 | tf_op jit(solution)/shard_map/dot_general | solution.py:169
  477.9 134.2 %all-gather.13.cloned.1.call-done = bf16[2048,2816]{1,0:T(8,128)(2,1)} async-done(((bf16[128,2816]{1,0:T(8,128)(2,1)}), bf16[2048,2816]{1,0:T(8,128)(2,1)}) %all-gather.13.cloned.1.call-update) | async-done | bytes 11534352 | tf_op jit(solution)/shard_map/all_gather | solution.py:82
  612.1 15.2 %convolution_convert_fusion = bf16[192,2048]{1,0:T(8,128)(2,1)} fusion(bf16[2816,2048]{0,1:T(8,128)(2,1)} %bitcast.79, bf16[192,2048]{1,0:T(8,128)(2,1)S(1)} %all_gather.26, bf16[2048,2816]{1,0:T(8,128)(2,1)} %all-gather.13.cloned.1.call-done, f32[192,2816]{1,0:T(8,128)} %fusion.27), kind=kOutput, calls=%fused_computation.19 | convolution fusion | flops 4432822272 | bytes 26804224 | tf_op jit(solution)/shard_map/dot_general | solution.py:172
  627.4 6.5 %reduce-scatter.5.cloned.1.call-done = bf16[96,2048]{1,0:T(8,128)(2,1)} async-done(((bf16[192,2048]{1,0:T(8,128)(2,1)}), bf16[96,2048]{1,0:T(8,128)(2,1)}) %reduce-scatter.5.cloned.1.call-update) | async-done | bytes 393232 | tf_op jit(solution)/shard_map/reduce_scatter | solution.py:173
  633.9 1.1 fusion.18
  635.0 2.4 all_gather.31
  637.3 0.9 copy.55
  (27 shorter events, 0.4 us)
Async XLA Ops:
  6.5 167.4 %copy-start = (bf16[512,2048]{1,0:T(8,128)(2,1)S(1)}, bf16[512,2048]{1,0:T(8,128)(2,1)}, u32[]{:S(2)}) copy-start(bf16[512,2048]{1,0:T(8,128)(2,1)} %param.18) | copy-start | bytes 6291460
  6.5 64.3 %all-gather.7.cloned.1.call-start = ((), (), s32[]{:S(2)}) async-start(), calls=%async_computation.2 | async-start | bytes 1671168 | tf_op jit(solution)/shard_map/all_gather | solution.py:150
  9.6 120.7 %all-gather.9.cloned.1.call-start = ((), (), s32[]{:S(2)}) async-start(), calls=%async_computation.3 | async-start | bytes 1671168 | tf_op jit(solution)/shard_map/all_gather | solution.py:151
  10.4 172.1 %reduce-scatter.3.cloned.1.call-start = ((), (), s32[]{:S(2)}) async-start(), calls=%async_computation.4 | async-start | bytes 1179648 | tf_op jit(solution)/shard_map/reduce_scatter | solution.py:156
  130.3 53.6 %copy-start.1 = (f32[2048]{0:T(1024)S(1)}, f32[2048]{0:T(1024)}, u32[]{:S(2)}) copy-start(f32[2048]{0:T(1024)} %param.20) | copy-start | bytes 24580
  175.4 152.2 %all-gather.15.cloned.1.call-start = ((), (), s32[]{:S(2)}) async-start(), calls=%async_computation.8 | async-start | bytes 12255232 | tf_op jit(solution)/shard_map/all_gather | solution.py:13
  176.0 293.9 %all-gather.11.cloned.1.call-start = ((), (), s32[]{:S(2)}) async-start(), calls=%async_computation.5 | async-start | bytes 12255232 | tf_op jit(solution)/shard_map/all_gather | solution.py:81
  176.6 435.5 %all-gather.13.cloned.1.call-start = ((), (), s32[]{:S(2)}) async-start(), calls=%async_computation.6 | async-start | bytes 12255232 | tf_op jit(solution)/shard_map/all_gather | solution.py:82
  177.2 456.7 %reduce-scatter.5.cloned.1.call-start = ((), (), s32[]{:S(2)}) async-start(), calls=%async_computation.7 | async-start | bytes 1179648 | tf_op jit(solution)/shard_map/reduce_scatter | solution.py:173
Sparse Core Ops, SparseCore 0:
  10.1 60.6 all-gather.6
  73.6 56.6 all-gather.8
  175.6 6.8 reduce-scatter.2
  185.1 142.5 all-gather.14
  330.2 139.5 all-gather.10
  472.5 139.5 all-gather.12
  627.5 6.3 reduce-scatter.4
